TPU v7x, 32 devices: a whole 2x2x4 slice. The times are simulated.
32 devices in a mesh: ep: 16 (over z, y, core), tp: 2 (over x).
Axes of the slice: x: 2, y: 2, z: 4, core: 2. Of those that a mesh axis runs over, the one named last changes fastest.
Arguments:
- tokens: bfloat16 [288, 1024], P('ep'), may hold values from -16 to 16
- delta_state: float32 [288, 4, 128, 128], P('ep', 'tp'), may hold values from -1.8 to 1.8
- mixer_gain: float32 [1024], replicated, may hold values from 0.1 to 1.9
- query_weight: bfloat16 [1024, 512], P(None, 'tp'), may hold values from -0.1875 to 0.1875
- key_weight: bfloat16 [1024, 512], P(None, 'tp'), may hold values from -0.1875 to 0.1875
- value_weight: bfloat16 [1024, 512], P(None, 'tp'), may hold values from -0.1875 to 0.1875
- write_weight: bfloat16 [1024, 4], P(None, 'tp'), may hold values from -0.1875 to 0.1875
- decay_weight: bfloat16 [1024, 4], P(None, 'tp'), may hold values from -0.1875 to 0.1875
- decay_rate: float32 [4], P('tp'), may hold values from 0.05 to 4
- decay_bias: float32 [4], P('tp'), may hold values from -2 to 1
- head_gain: float32 [128], replicated, may hold values from 0.1 to 1.9
- out_weight: bfloat16 [512, 1024], P('tp'), may hold values from -0.25 to 0.25
- channel_gain: float32 [1024], replicated, may hold values from 0.1 to 1.9
- routes: int32 [288, 6], P('ep'), may hold values from 0 to 15, all different within a row; in each aligned block of 18 rows (0 to 17, 18 to 35, ...) at most 13 rows name the same one
- route_weights: float32 [288, 6], P('ep'), may hold values from 0.1 to 1
- expert_gate: bfloat16 [16, 1024, 512], P('ep', None, 'tp'), may hold values from -0.1875 to 0.1875
- expert_up: bfloat16 [16, 1024, 512], P('ep', None, 'tp'), may hold values from -0.1875 to 0.1875
- expert_down: bfloat16 [16, 512, 1024], P('ep', 'tp'), may hold values from -0.25 to 0.25
- shared_gate: bfloat16 [1024, 512], P(None, 'tp'), may hold values from -0.1875 to 0.1875
- shared_up: bfloat16 [1024, 512], P(None, 'tp'), may hold values from -0.1875 to 0.1875
- shared_down: bfloat16 [512, 1024], P('tp'), may hold values from -0.25 to 0.25
Outputs:
- layer_out: bfloat16 [288, 1024], P('ep', 'tp')
- next_state: float32 [288, 4, 128, 128], P('ep', 'tp')
Inputs may be any that keep to these rules, and one draw needn't show every extreme that they name: `routes`: each row names 6 different experts. In each aligned block of 18 rows (the rows of one ep index) no expert is named by more than 13 rows, a bound that some block reaches.
All inputs are finite; a program needn't handle non-finite values.
Results may differ from a plain program's by a relative error of at most 0.015.
Values may be sent and summed in bfloat16 or wider, within the bound.
A program may use at most 64 MiB of HBM per device.

v0:
```python
import jax
import jax.numpy as jnp
from jax import lax
from jax.sharding import PartitionSpec as P

EPS = 1e-06
ROUTED_SCALE = 2.5


def rms_rows(values, gain_vec):
    mean_square = jnp.mean(values * values, axis=-1, keepdims=True)
    return values * lax.rsqrt(mean_square + EPS) * gain_vec


def unit_heads(raw, heads, head_dim):
    shaped = raw.astype(jnp.float32).reshape(raw.shape[0], heads, head_dim)
    return shaped * lax.rsqrt(jnp.sum(shaped * shaped, axis=-1, keepdims=True) + EPS)


def per_device(
    tokens,
    delta_state,
    mixer_gain,
    query_weight,
    key_weight,
    value_weight,
    write_weight,
    decay_weight,
    decay_rate,
    decay_bias,
    head_gain,
    out_weight,
    channel_gain,
    routes,
    route_weights,
    expert_gate,
    expert_up,
    expert_down,
    shared_gate,
    shared_up,
    shared_down,
):
    seq_rows, model_width = tokens.shape
    heads, head_dim = (delta_state.shape[1], delta_state.shape[2])
    top_k = routes.shape[1]
    tp_count = lax.axis_size("tp")
    ep_count = lax.axis_size("ep")
    share_width = model_width // tp_count
    share_start = lax.axis_index("tp") * share_width
    exp_local = expert_gate.shape[0]
    expert_total = exp_local * ep_count
    capacity = max(2, min(seq_rows, 2 * seq_rows * top_k // expert_total))
    pair_count = seq_rows * top_k
    normed = rms_rows(tokens.astype(jnp.float32), mixer_gain).astype(jnp.bfloat16)
    query_raw = jnp.dot(normed, query_weight, preferred_element_type=jnp.float32).astype(
        jnp.bfloat16
    )
    key_raw = jnp.dot(normed, key_weight, preferred_element_type=jnp.float32).astype(jnp.bfloat16)
    value_raw = jnp.dot(normed, value_weight, preferred_element_type=jnp.float32).astype(
        jnp.bfloat16
    )
    write_rate = jax.nn.sigmoid(jnp.dot(normed, write_weight, preferred_element_type=jnp.float32))
    decay_keep = jnp.exp(
        -decay_rate
        * jax.nn.softplus(
            jnp.dot(normed, decay_weight, preferred_element_type=jnp.float32) + decay_bias
        )
    )
    query_unit = unit_heads(query_raw, heads, head_dim) * head_dim ** (-0.5)
    key_unit = unit_heads(key_raw, heads, head_dim)
    value_vec = value_raw.astype(jnp.float32).reshape(seq_rows, heads, head_dim)
    held_state = decay_keep[:, :, None, None] * delta_state
    correction = value_vec - jnp.einsum(
        "rhkv,rhk->rhv", held_state, key_unit, precision=lax.Precision.HIGHEST
    )
    next_state = (
        held_state
        + write_rate[:, :, None, None] * key_unit[:, :, :, None] * correction[:, :, None, :]
    )
    readout = jnp.einsum("rhkv,rhk->rhv", next_state, query_unit, precision=lax.Precision.HIGHEST)
    head_out = rms_rows(readout, head_gain).astype(jnp.bfloat16).reshape(seq_rows, heads * head_dim)
    head_partial = jnp.dot(head_out, out_weight, preferred_element_type=jnp.float32)
    head_partial = head_partial.astype(jnp.bfloat16).astype(jnp.float32)
    mixer_out = lax.psum(head_partial.astype(jnp.bfloat16), "tp")
    residual = (tokens.astype(jnp.float32) + mixer_out.astype(jnp.float32)).astype(jnp.bfloat16)
    expert_input = rms_rows(residual.astype(jnp.float32), channel_gain).astype(jnp.bfloat16)
    residual_share = lax.dynamic_slice_in_dim(residual, share_start, share_width, 1)
    weight_norm = route_weights / jnp.sum(route_weights, axis=1, keepdims=True) * ROUTED_SCALE
    shared_act = (
        jax.nn.silu(jnp.dot(expert_input, shared_gate, preferred_element_type=jnp.float32))
        * jnp.dot(expert_input, shared_up, preferred_element_type=jnp.float32)
    ).astype(jnp.bfloat16)
    shared_partial = jnp.dot(shared_act, shared_down, preferred_element_type=jnp.float32)
    shared_partial = shared_partial.astype(jnp.bfloat16).astype(jnp.float32)
    order_pos = jnp.arange(pair_count, dtype=jnp.int32)
    pair_ids = routes.reshape(pair_count)
    earlier = (pair_ids[:, None] == pair_ids[None, :]) & (order_pos[:, None] > order_pos[None, :])
    slot_index = jnp.sum(earlier.astype(jnp.int32), axis=1)
    slot_flat = pair_ids * capacity + slot_index
    slot_total = expert_total * capacity
    slot_iota = jnp.arange(slot_total, dtype=jnp.int32)
    hit_table = (slot_iota[:, None] == slot_flat[None, :]).astype(jnp.float32)
    dispatch = jnp.sum(hit_table.reshape(slot_total, seq_rows, top_k), axis=2).astype(jnp.bfloat16)
    combine_mat = jnp.sum(
        (hit_table * weight_norm.reshape(1, pair_count)).reshape(slot_total, seq_rows, top_k),
        axis=2,
    )
    outgoing = jnp.dot(dispatch, expert_input, preferred_element_type=jnp.float32).astype(
        jnp.bfloat16
    )
    outgoing = outgoing.reshape(ep_count, exp_local * capacity, model_width)
    received = lax.all_to_all(outgoing, "ep", split_axis=0, concat_axis=0, tiled=True)
    expert_rows = received.reshape(ep_count, exp_local, capacity, model_width).transpose(1, 0, 2, 3)
    expert_rows = expert_rows.reshape(exp_local, ep_count * capacity, model_width)
    gate_val = jnp.einsum(
        "lrd,ldf->lrf", expert_rows, expert_gate, preferred_element_type=jnp.float32
    )
    up_val = jnp.einsum("lrd,ldf->lrf", expert_rows, expert_up, preferred_element_type=jnp.float32)
    hidden_act = (jax.nn.silu(gate_val) * up_val).astype(jnp.bfloat16)
    down_part = jnp.einsum(
        "lrf,lfd->lrd", hidden_act, expert_down, preferred_element_type=jnp.float32
    )
    down_part = down_part.astype(jnp.bfloat16).astype(jnp.float32).reshape(-1, model_width)
    summed, shared_sum = (
        lax.psum_scatter(
            down_part.astype(jnp.bfloat16), "tp", scatter_dimension=1, tiled=True
        ).astype(jnp.float32),
        lax.psum_scatter(
            shared_partial.astype(jnp.bfloat16), "tp", scatter_dimension=1, tiled=True
        ).astype(jnp.float32),
    )
    expert_share = summed.astype(jnp.bfloat16).reshape(exp_local, ep_count, capacity, share_width)
    shared_out = shared_sum.astype(jnp.bfloat16)
    homeward = expert_share.transpose(1, 0, 2, 3).reshape(
        ep_count, exp_local * capacity, share_width
    )
    returned = lax.all_to_all(homeward, "ep", split_axis=0, concat_axis=0, tiled=True)
    routed = jnp.einsum(
        "ts,td->sd",
        combine_mat,
        returned.reshape(slot_total, share_width).astype(jnp.float32),
        precision=lax.Precision.HIGHEST,
    )
    layer_out = (
        residual_share.astype(jnp.float32) + routed + shared_out.astype(jnp.float32)
    ).astype(jnp.bfloat16)
    return (layer_out, next_state)


def solution(mesh):
    return jax.shard_map(
        per_device,
        mesh=mesh,
        in_specs=(
            P("ep", None),
            P("ep", "tp", None, None),
            P(),
            P(None, "tp"),
            P(None, "tp"),
            P(None, "tp"),
            P(None, "tp"),
            P(None, "tp"),
            P("tp"),
            P("tp"),
            P(),
            P("tp", None),
            P(),
            P("ep", None),
            P("ep", None),
            P("ep", None, "tp"),
            P("ep", None, "tp"),
            P("ep", "tp", None),
            P(None, "tp"),
            P(None, "tp"),
            P("tp", None),
        ),
        out_specs=(P("ep", "tp"), P("ep", "tp", None, None)),
        check_vma=False,
    )
```

profile of v0, /device:TPU:0, one launch (start us, length us, event | category | flops | bytes accessed | tf_op | source)
XLA Modules:
  0.0 100.9 jit_solution(10764889554871645032)
XLA Ops:
  7.2 0.9 copy.35
  8.5 0.7 reduce_sum.89
  9.3 0.7 divide_multiply_fusion
  10.0 0.9 fusion.27
  11.0 1.3 %fusion.8 = f32[18,256]{1,0:T(8,128)S(1)} fusion(bf16[1024,256]{1,0:T(8,128)(2,1)} %param.26, bf16[18,1024]{1,0:T(8,128)(2,1)} %param.21, f32[1024]{0:T(1024)} %param.23, f32[18]{0:T(128)S(1)} %add_rsqrt_fusion.4), kind=kOutput, calls=%fused_computation.18 | convolution fusion | flops 9520128 | bytes 583752 | tf_op jit(solution)/shard_map/dot_general | solution.py:59
  12.3 1.0 %fusion.12 = f32[18,2]{0,1:T(2,128)S(1)} fusion(bf16[1024,2]{0,1:T(2,128)(2,1)} %param.27, bf16[18,1024]{1,0:T(8,128)(2,1)} %param.21, f32[1024]{0:T(1024)} %param.23, f32[18]{0:T(128)S(1)} %add_rsqrt_fusion.4), kind=kOutput, calls=%fused_computation.25 | convolution fusion | flops 147564 | bytes 45272 | tf_op jit(solution)/shard_map/dot_general | solution.py:62
  13.4 1.3 %fusion.9 = f32[18,256]{1,0:T(8,128)S(1)} fusion(bf16[1024,256]{1,0:T(8,128)(2,1)} %param.25, bf16[18,1024]{1,0:T(8,128)(2,1)} %param.21, f32[1024]{0:T(1024)} %param.23, f32[18]{0:T(128)S(1)} %add_rsqrt_fusion.4), kind=kOutput, calls=%fused_computation.20 | convolution fusion | flops 9520128 | bytes 583752 | tf_op jit(solution)/shard_map/dot_general | solution.py:58
  14.9 0.7 neg.19
  15.6 1.0 %fusion.40 = f32[18,2]{0,1:T(2,128)S(1)} fusion(bf16[1024,2]{0,1:T(2,128)(2,1)} %param.28, f32[2]{0:T(128)} %param.30, f32[2]{0:T(128)S(1)} %neg.19, bf16[18,1024]{1,0:T(8,128)(2,1)} %param.21, f32[1024]{0:T(1024)} %param.23, f32[18]{0:T(128)S(1)} %add_rsqrt_fusion.4), kind=kOutput, calls=%fused_computation.75 | convolution fusion | flops 147744 | bytes 45288 | tf_op jit(solution)/shard_map/dot_general | solution.py:66
  16.7 1.3 %fusion.7 = f32[18,256]{1,0:T(8,128)S(1)} fusion(bf16[1024,256]{1,0:T(8,128)(2,1)} %param.24, bf16[18,1024]{1,0:T(8,128)(2,1)} %param.21, f32[1024]{0:T(1024)} %param.23, f32[18]{0:T(128)S(1)} %add_rsqrt_fusion.4), kind=kOutput, calls=%fused_computation.16 | convolution fusion | flops 9520128 | bytes 583752 | tf_op jit(solution)/shard_map/dot_general | solution.py:55
  18.4 2.2 %fusion = f32[18,2,1,128]{3,2,1,0:T(1,128)S(1)} fusion(f32[18,2,128,1]{2,3,1,0:T(1,128)S(1)} %bitcast.44, f32[18,2,128,128]{3,2,1,0:T(8,128)S(1)} %copy-done.1, f32[18,2]{1,0:T(8,128)S(1)} %copy.33), kind=kOutput, calls=%fused_computation.1 | convolution fusion | flops 7667712 | bytes 2396304 | tf_op jit(solution)/shard_map/rhkv,rhk->rhv/dot_general | solution.py:73
  20.6 0.8 multiply_add_fusion
  21.5 1.3 %copy-done.2 = f32[18,2,128,128]{3,2,1,0:T(8,128)} copy-done((f32[18,2,128,128]{3,2,1,0:T(8,128)}, f32[18,2,128,128]{3,2,1,0:T(8,128)S(1)}, u32[]{:S(2)}) %copy-start.2) | copy-done | bytes 2359320
  22.9 2.1 %fusion.54 = f32[18,2,1,128]{3,2,1,0:T(1,128)S(1)} fusion(f32[18,2,128,128]{3,2,1,0:T(8,128)S(1)} %multiply_add_fusion, f32[18,2,128,1]{2,3,1,0:T(1,128)S(1)} %bitcast.43), kind=kOutput, calls=%fused_computation.81 | convolution fusion | flops 7077888 | bytes 2396160 | tf_op jit(solution)/shard_map/rhkv,rhk->rhv/dot_general | solution.py:80
  25.4 10.2 %psum.7 = bf16[18,1024]{1,0:T(8,128)(2,1)S(1)} all-reduce(bf16[18,1024]{1,0:T(8,128)(2,1)S(1)} %convolution_convert_fusion.3), channel_id=1, replica_groups=mesh['ep'=16,'tp'=2] {'tp'}, use_global_device_ids=true, to_apply=%region_4.5 | all-reduce | flops 18432 | bytes 73728 | tf_op jit(solution)/shard_map/psum | solution.py:84
  36.5 19.9 %all_to_all.10 = bf16[16,13,1024]{2,1,0:T(8,128)(2,1)S(1)} all-to-all(bf16[16,13,1024]{2,1,0:T(8,128)(2,1)S(1)} %reshape.159), channel_id=1, replica_groups=mesh['ep'=16,'tp'=2] {'ep'}, dimensions={0} | all-to-all | bytes 851968 | tf_op jit(solution)/shard_map/all_to_all | solution.py:112
  56.9 2.5 %convolution_convert_fusion = bf16[208,1024]{1,0:T(8,128)(2,1)} fusion(bf16[208,1024]{1,0:T(8,128)(2,1)S(1)} %reshape.160, bf16[1,256,1024]{2,1,0:T(8,128)(2,1)S(1)} %copy-done, bf16[1,1024,256]{2,1,0:T(8,128)(2,1)} %param.37, f32[208,256]{1,0:T(8,128)S(1)} %fusion.16), kind=kOutput, calls=%fused_computation.3 | convolution fusion | flops 218636288 | bytes 2113536 | tf_op jit(solution)/shard_map/lrf,lfd->lrd/dot_general | solution.py:120
  59.4 12.3 %reduce-scatter.3.cloned.1.call-done = bf16[208,512]{1,0:T(8,128)(2,1)} async-done(((bf16[208,1024]{1,0:T(8,128)(2,1)}), bf16[208,512]{1,0:T(8,128)(2,1)}) %reduce-scatter.3.cloned.1.call-update) | async-done | bytes 213008 | tf_op jit(solution)/shard_map/reduce_scatter | solution.py:125
  71.7 1.7 %reshape_transpose_reshape.4 = bf16[16,13,512]{2,1,0:T(8,128)(2,1)} reshape(bf16[208,512]{1,0:T(8,128)(2,1)} %reduce-scatter.3.cloned.1.call-done) | data formatting | bytes 425984 | tf_op jit(solution)/shard_map/reshape;transpose;reshape | solution.py:134
  73.4 5.6 %all-to-all-start.1 = ((bf16[16,13,512]{2,1,0:T(8,128)(2,1)}), bf16[16,13,512]{2,1,0:T(8,128)(2,1)S(1)}, u32[]{:S(2)}, u32[]{:S(2)}) async-start(bf16[16,13,512]{2,1,0:T(8,128)(2,1)} %reshape_transpose_reshape.4), calls=%async_computation.2 | async-start | bytes 524288 | tf_op jit(solution)/shard_map/all_to_all | solution.py:137
  79.4 1.1 %convolution_convert_fusion.2 = bf16[18,1024]{1,0:T(8,128)(2,1)} fusion(bf16[256,1024]{1,0:T(8,128)(2,1)S(1)} %copy-done.7, bf16[1024,256]{1,0:T(8,128)(2,1)S(1)} %copy-done.8, f32[18,256]{1,0:T(8,128)S(1)} %fusion.45, bf16[18,1024]{1,0:T(8,128)(2,1)S(1)} %get-tuple-element.5, f32[1024]{0:T(1024)S(1)} %copy-done.9, f32[18]{0:T(128)S(1)} %add_rsqrt_fusion.3), kind=kOutput, calls=%fused_computation.8 | convolution fusion | flops 18994176 | bytes 1144904 | tf_op jit(solution)/shard_map/dot_general | solution.py:93
  80.5 8.5 %all-to-all-done.1 = bf16[16,13,512]{2,1,0:T(8,128)(2,1)S(1)} async-done(((bf16[16,13,512]{2,1,0:T(8,128)(2,1)}), bf16[16,13,512]{2,1,0:T(8,128)(2,1)S(1)}, u32[]{:S(2)}, u32[]{:S(2)}) %all-to-all-start.1) | async-done | bytes 213024 | tf_op jit(solution)/shard_map/all_to_all | solution.py:137
  89.2 3.3 %reduce-scatter.5.cloned.1.call-done = bf16[18,512]{1,0:T(8,128)(2,1)} async-done(((bf16[18,1024]{1,0:T(8,128)(2,1)}), bf16[18,512]{1,0:T(8,128)(2,1)}) %reduce-scatter.5.cloned.1.call-update) | async-done | bytes 18448 | tf_op jit(solution)/shard_map/reduce_scatter | solution.py:128
  92.5 1.6 %fusion.5 = bf16[18,512]{1,0:T(8,128)(2,1)} fusion(f32[208,18]{0,1:T(8,128)S(1)} %get-tuple-element.3, bf16[208,512]{1,0:T(8,128)(2,1)S(1)} %reshape.164, bf16[18,512]{1,0:T(8,128)(2,1)} %reduce-scatter.5.cloned.1.call-done, bf16[18,1024]{1,0:T(8,128)(2,1)S(1)} %get-tuple-element.5, s32[]{:T(128)S(6)} %select_n.8), kind=kOutput, calls=%fused_computation.12 | convolution fusion | flops 23049216 | bytes 283268 | tf_op jit(solution)/shard_map/ts,td->sd/dot_general | solution.py:138
  (58 shorter events, 3.2 us)
Async XLA Ops:
  7.2 49.7 %copy-start = (bf16[1,256,1024]{2,1,0:T(8,128)(2,1)S(1)}, bf16[1,256,1024]{2,1,0:T(8,128)(2,1)}, u32[]{:S(2)}) copy-start(bf16[1,256,1024]{2,1,0:T(8,128)(2,1)} %param.38) | copy-start | bytes 1572868
  7.2 11.2 %copy-start.1 = (f32[18,2,128,128]{3,2,1,0:T(8,128)S(1)}, f32[18,2,128,128]{3,2,1,0:T(8,128)}, u32[]{:S(2)}) copy-start(f32[18,2,128,128]{3,2,1,0:T(8,128)} %param.22) | copy-start | bytes 7077892
  7.2 64.5 %reduce-scatter.3.cloned.1.call-start = ((), (), s32[]{:S(2)}) async-start(), calls=%async_computation.4 | async-start | bytes 638976 | tf_op jit(solution)/shard_map/reduce_scatter | solution.py:125
  21.5 1.4 %copy-start.2 = (f32[18,2,128,128]{3,2,1,0:T(8,128)}, f32[18,2,128,128]{3,2,1,0:T(8,128)S(1)}, u32[]{:S(2)}) copy-start(f32[18,2,128,128]{3,2,1,0:T(8,128)S(1)} %multiply_add_fusion) | copy-start | bytes 7077892
  21.5 3.6 %copy-start.10 = (f32[128]{0:T(128)S(1)}, f32[128]{0:T(128)}, u32[]{:S(2)}) copy-start(f32[128]{0:T(128)} %param.31) | copy-start | bytes 1540
  21.5 3.7 %copy-start.4 = (bf16[256,1024]{1,0:T(8,128)(2,1)S(1)}, bf16[256,1024]{1,0:T(8,128)(2,1)}, u32[]{:S(2)}) copy-start(bf16[256,1024]{1,0:T(8,128)(2,1)} %param.32) | copy-start | bytes 1572868
  21.5 14.2 %copy-start.3 = (bf16[18,1024]{1,0:T(8,128)(2,1)S(1)}, bf16[18,1024]{1,0:T(8,128)(2,1)}, u32[]{:S(2)}) copy-start(bf16[18,1024]{1,0:T(8,128)(2,1)} %param.21) | copy-start | bytes 110596
  21.5 14.5 %copy-start.9 = (f32[1024]{0:T(1024)S(1)}, f32[1024]{0:T(1024)}, u32[]{:S(2)}) copy-start(f32[1024]{0:T(1024)} %param.33) | copy-start | bytes 12292
  25.0 31.5 %copy-start.5 = (bf16[1,1024,256]{2,1,0:T(8,128)(2,1)S(1)}, bf16[1,1024,256]{2,1,0:T(8,128)(2,1)}, u32[]{:S(2)}) copy-start(bf16[1,1024,256]{2,1,0:T(8,128)(2,1)} %param.36) | copy-start | bytes 1572868
  56.5 22.6 %copy-start.6 = (bf16[1024,256]{1,0:T(8,128)(2,1)S(1)}, bf16[1024,256]{1,0:T(8,128)(2,1)}, u32[]{:S(2)}) copy-start(bf16[1024,256]{1,0:T(8,128)(2,1)} %param.39) | copy-start | bytes 1572868
  56.8 22.5 %copy-start.7 = (bf16[256,1024]{1,0:T(8,128)(2,1)S(1)}, bf16[256,1024]{1,0:T(8,128)(2,1)}, u32[]{:S(2)}) copy-start(bf16[256,1024]{1,0:T(8,128)(2,1)} %param.41) | copy-start | bytes 1572868
  56.8 22.5 %copy-start.8 = (bf16[1024,256]{1,0:T(8,128)(2,1)S(1)}, bf16[1024,256]{1,0:T(8,128)(2,1)}, u32[]{:S(2)}) copy-start(bf16[1024,256]{1,0:T(8,128)(2,1)} %param.40) | copy-start | bytes 1572868
  73.4 15.6 %all-to-all-start.1 = ((bf16[16,13,512]{2,1,0:T(8,128)(2,1)}), bf16[16,13,512]{2,1,0:T(8,128)(2,1)S(1)}, u32[]{:S(2)}, u32[]{:S(2)}) async-start(bf16[16,13,512]{2,1,0:T(8,128)(2,1)} %reshape_transpose_reshape.4), calls=%async_computation.2 | async-start | bytes 524288 | tf_op jit(solution)/shard_map/all_to_all | solution.py:137
  79.0 13.4 %reduce-scatter.5.cloned.1.call-start = ((), (), s32[]{:S(2)}) async-start(), calls=%async_computation.5 | async-start | bytes 73728 | tf_op jit(solution)/shard_map/reduce_scatter | solution.py:128
Sparse Core Ops, SparseCore 0:
  59.5 12.1 reduce-scatter.2
  82.1 10.3 reduce-scatter.4
where the time goes:
time: 102 us; the launch traced here: 101 us
  blocking collectives  30.1 us (30%)
  waiting for transfers between devices  24.2 us (24%)
  matrix products  16.6 us (16%)
  between operations  14.4 us (14%)
  starting transfers between devices  5.7 us (6%)
  local copies, waits for them, and re-layouts  4.98 us (5%)
  other arithmetic  4.91 us (5%)
    all_to_all x1, blocking collectives, per_device(): lax.all_to_all(outgoing, 'ep', split_axis=0, concat_axis=0, tiled=True)  19.9 us
    reduce_scatter x1, waiting for transfers between devices, per_device(): lax.psum_scatter(down_part.astype(jnp.bfloat16), 'tp', scatter_dimension=...  12.3 us
    psum x1, blocking collectives, per_device(): mixer_out = lax.psum(head_partial.astype(jnp.bfloat16), 'tp')  10.2 us
    all_to_all x1, waiting for transfers between devices, per_device(): lax.all_to_all(homeward, 'ep', split_axis=0, concat_axis=0, tiled=True)  8.54 us
    all_to_all x1, starting transfers between devices, per_device(): lax.all_to_all(homeward, 'ep', split_axis=0, concat_axis=0, tiled=True)  5.62 us
    reduce_scatter x1, waiting for transfers between devices, per_device(): lax.psum_scatter(shared_partial.astype(jnp.bfloat16), 'tp', scatter_dimen...  3.32 us
    dot_general x1, matrix products, per_device(): jnp.einsum('lrf,lfd->lrd', hidden_act, expert_down, preferred_element_typ...  2.54 us
    unnamed x25, local copies, waits for them, and re-layouts  2.36 us
  transfers between devices with their start and end apart: 3, of which 3 were waited for; matrix products, arithmetic and copies ran while one was open for 1% of the time, Pallas kernels for 0%

commit v1 on v0

v1 whole, which is shorter than its diff:
```python
import functools

import jax
import jax.numpy as jnp
from jax import lax
from jax.experimental import pallas as pl
from jax.experimental.pallas import tpu as pltpu
from jax.sharding import PartitionSpec as P

EPS = 1e-06
ROUTED_SCALE = 2.5
MESH = pl.DeviceIdType.MESH
F32 = jnp.float32
BF16 = jnp.bfloat16


def rms_rows(values, gain_row):
    mean_square = jnp.mean(values * values, axis=-1, keepdims=True)
    return values * lax.rsqrt(mean_square + EPS) * gain_row


def round_up(value, step):
    return -(-value // step) * step


def mixer_kernel(
    expert_total, chunk,
    tokens_ref, mixer_gain_ref, write_ref, decay_ref, rate_ref, bias_ref,
    head_gain_ref, routes_ref, route_weights_ref,
    state_hbm, query_hbm, key_hbm, value_hbm, out_hbm,
    next_hbm, partial_ref, wext_ref,
    state, query_w, key_w, value_w, out_w, columns, readout,
    weight_sems, in_sems, out_sems,
):
    rows, heads, dim = state.shape[0], state.shape[1], state.shape[2]
    chunks = rows // chunk
    weights = [
        pltpu.make_async_copy(src, dst, weight_sems.at[i])
        for i, (src, dst) in enumerate(
            ((key_hbm, key_w), (query_hbm, query_w), (value_hbm, value_w), (out_hbm, out_w))
        )
    ]
    loads = [
        pltpu.make_async_copy(
            state_hbm.at[pl.ds(i * chunk, chunk)], state.at[pl.ds(i * chunk, chunk)], in_sems.at[i]
        )
        for i in range(chunks)
    ]
    stores = [
        pltpu.make_async_copy(
            state.at[pl.ds(i * chunk, chunk)], next_hbm.at[pl.ds(i * chunk, chunk)], out_sems.at[i]
        )
        for i in range(chunks)
    ]
    for copy in weights[:3] + loads + weights[3:]:
        copy.start()

    raw = route_weights_ref[...]
    norm = raw / jnp.sum(raw, axis=1, keepdims=True) * ROUTED_SCALE
    routes = routes_ref[...]
    lane = lax.broadcasted_iota(jnp.int32, (rows, wext_ref.shape[1]), 1)
    high = jnp.zeros(lane.shape, F32)
    for k in range(routes.shape[1]):
        hit = (lane == routes[:, k : k + 1]) | (lane == routes[:, k : k + 1] + expert_total)
        high = high + jnp.where(hit, norm[:, k : k + 1], 0.0)
    rounded = high.astype(BF16)
    low = (high - rounded.astype(F32)).astype(BF16)
    wext_ref[...] = jnp.where(lane < expert_total, rounded.astype(F32), low.astype(F32)).astype(BF16)

    normed = rms_rows(tokens_ref[...].astype(F32), mixer_gain_ref[...]).astype(BF16)
    write_rate = jax.nn.sigmoid(jnp.dot(normed, write_ref[...], preferred_element_type=F32))
    pre = jnp.dot(normed, decay_ref[...], preferred_element_type=F32) + bias_ref[...]
    softplus = jnp.maximum(pre, 0.0) + jnp.log1p(jnp.exp(-jnp.abs(pre)))
    keep = jnp.exp(-rate_ref[...] * softplus)

    def project(copy, ref):
        copy.wait()
        return jnp.dot(normed, ref[...], preferred_element_type=F32).astype(BF16).astype(F32)

    key_raw = project(weights[0], key_w)
    query_raw = project(weights[1], query_w)
    value_raw = project(weights[2], value_w)
    stride = round_up(rows, 8)
    per_head = []
    for h in range(heads):
        part = slice(h * dim, (h + 1) * dim)
        k_h, q_h = key_raw[:, part], query_raw[:, part]
        k_h = k_h * lax.rsqrt(jnp.sum(k_h * k_h, axis=-1, keepdims=True) + EPS)
        q_h = q_h * lax.rsqrt(jnp.sum(q_h * q_h, axis=-1, keepdims=True) + EPS) * dim ** (-0.5)
        columns[2 * h * stride : 2 * h * stride + rows, :] = k_h
        columns[(2 * h + 1) * stride : (2 * h + 1) * stride + rows, :] = q_h
        dots = jnp.sum(k_h * q_h, axis=-1, keepdims=True)
        per_head.append(
            (
                value_raw[:, part],
                jnp.broadcast_to(keep[:, h : h + 1], (rows, dim)),
                jnp.broadcast_to(write_rate[:, h : h + 1], (rows, dim)),
                jnp.broadcast_to(dots, (rows, dim)),
            )
        )
    turned = columns[...].T

    for i in range(chunks):
        loads[i].wait()
        for r in range(i * chunk, (i + 1) * chunk):
            for h in range(heads):
                v_h, keep_h, write_h, dots_h = (x[r : r + 1, :] for x in per_head[h])
                at = 2 * h * stride + r
                k_col = jnp.broadcast_to(turned[:, at : at + 1], (dim, dim))
                q_col = jnp.broadcast_to(turned[:, at + stride : at + stride + 1], (dim, dim))
                old = state[r, h]
                seen = jnp.sum(old * k_col, axis=0, keepdims=True)
                asked = jnp.sum(old * q_col, axis=0, keepdims=True)
                step = write_h * (v_h - keep_h * seen)
                state[r, h] = keep_h * old + k_col * step
                readout[r : r + 1, h * dim : (h + 1) * dim] = keep_h * asked + dots_h * step
        stores[i].start()

    weights[3].wait()
    total = jnp.zeros(partial_ref.shape, F32)
    for h in range(heads):
        part = slice(h * dim, (h + 1) * dim)
        head_out = rms_rows(readout[:, part], head_gain_ref[...]).astype(BF16)
        total = total + jnp.dot(head_out, out_w[part, :], preferred_element_type=F32)
    partial_ref[...] = total.astype(BF16)
    for copy in stores:
        copy.wait()


def flip(index, mask):
    bit = 1
    while bit <= mask:
        if mask & bit:
            index = index + bit - 2 * bit * ((index // bit) % 2)
        bit *= 2
    return index


def experts_kernel(
    zs, ys, tps, pad,
    tokens_ref, partial_ref, wext_ref, channel_gain_ref,
    gate_hbm, up_hbm, down_hbm, sgate_hbm, sup_hbm, sdown_hbm,
    out_ref,
    gate_w, up_w, down_w, sgate_w, sup_w, sdown_w,
    mixed, blocks, packed, near, core_send, core_recv, y_send, y_recv,
    z_send, z_recv, own_share,
    weight_sems, x_send_sems, x_recv_sems,
    agz_send_sems, agz_recv_sems, agy_send_sems, agy_recv_sems,
    agc_send_sems, agc_recv_sems,
    rsc_send_sems, rsc_recv_sems, rsy_send_sems, rsy_recv_sems,
    rsz_send_sems, rsz_recv_sems,
):
    rows, width = tokens_ref.shape
    share = width // tps
    me, tp = lax.axis_index("ep"), lax.axis_index("tp")
    core, chip = me % 2, me // 2
    y, z = chip % ys, chip // ys
    expert_total = 2 * ys * zs

    def ep_of(dz, dy, dc):
        return (flip(z, dz) * ys + flip(y, dy)) * 2 + flip(core, dc)

    weights = [
        pltpu.make_async_copy(src, dst, weight_sems.at[i])
        for i, (src, dst) in enumerate(
            (
                (sgate_hbm, sgate_w), (sup_hbm, sup_w), (sdown_hbm, sdown_w),
                (gate_hbm, gate_w), (up_hbm, up_w), (down_hbm, down_w),
            )
        )
    ]
    for copy in weights:
        copy.start()

    peers = [(ep_of(dz, 0, 0), flip(tp, dt)) for dz in range(zs) for dt in range(tps) if dz or dt]
    peers += [(ep_of(0, dy, 0), tp) for dy in range(1, ys)] + [(ep_of(0, 0, 1), tp)]
    barrier = pltpu.get_barrier_semaphore()
    for peer in peers:
        pl.semaphore_signal(barrier, inc=1, device_id=peer, device_id_type=MESH)
    pl.semaphore_wait(barrier, len(peers))

    def remote(src, dst, send_sem, recv_sem, peer):
        copy = pltpu.make_async_remote_copy(
            src_ref=src, dst_ref=dst, send_sem=send_sem, recv_sem=recv_sem,
            device_id=peer, device_id_type=MESH,
        )
        copy.start()
        return copy

    sent = []

    x_copies = [
        remote(partial_ref, mixed.at[dt - 1], x_send_sems.at[dt - 1], x_recv_sems.at[dt - 1],
               (me, flip(tp, dt)))
        for dt in range(1, tps)
    ]
    mixer_out = partial_ref[...].astype(F32)
    for dt in range(1, tps):
        x_copies[dt - 1].wait_recv()
        mixer_out = mixer_out + mixed[dt - 1].astype(F32)
    sent += x_copies
    mixer_out = mixer_out.astype(BF16).astype(F32)
    residual = (tokens_ref[...].astype(F32) + mixer_out).astype(BF16)
    expert_input = rms_rows(residual.astype(F32), channel_gain_ref[...]).astype(BF16)
    for t in range(tps):
        own_share[t] = residual[:, t * share : (t + 1) * share].astype(F32)
    blocks[0, :, :width] = expert_input
    blocks[0, :, width:] = wext_ref[...]

    def slot(dz, dy, dc):
        return (dc * zs + dz) * ys + dy

    z_copies = {
        dz: remote(blocks.at[slot(0, 0, 0)], blocks.at[slot(dz, 0, 0)],
                   agz_send_sems.at[dz], agz_recv_sems.at[dz], (ep_of(dz, 0, 0), tp))
        for dz in range(1, zs)
    }
    y_copies, c_copies = {}, {}

    def to_core(dz, dy):
        at = dz * ys + dy
        c_copies[dz, dy] = remote(
            blocks.at[slot(dz, dy, 0)], blocks.at[slot(dz, dy, 1)],
            agc_send_sems.at[at], agc_recv_sems.at[at], (ep_of(0, 0, 1), tp))

    def pack(dz, dy, dc):
        at = slot(dz, dy, dc)
        packed[at * pad : at * pad + rows, :] = blocks[at]

    def pass_on(dz):
        for dy in range(1, ys):
            at = dz * ys + dy
            y_copies[dz, dy] = remote(
                blocks.at[slot(dz, 0, 0)], blocks.at[slot(dz, dy, 0)],
                agy_send_sems.at[at], agy_recv_sems.at[at], (ep_of(0, dy, 0), tp))
        to_core(dz, 0)

    pass_on(0)

    for copy in weights[:3]:
        copy.wait()

    def gated(x, g_ref, u_ref):
        g = jnp.dot(x, g_ref[...], preferred_element_type=F32)
        u = jnp.dot(x, u_ref[...], preferred_element_type=F32)
        return (g * jax.nn.sigmoid(g) * u).astype(BF16)

    shared_act = gated(expert_input, sgate_w, sup_w)
    shared_part = jnp.dot(shared_act, sdown_w[...], preferred_element_type=F32)
    pack(0, 0, 0)
    for copy in weights[3:]:
        copy.wait()

    for dz in range(1, zs):
        z_copies[dz].wait_recv()
        pass_on(dz)
        pack(dz, 0, 0)
    for dz in range(zs):
        for dy in range(1, ys):
            y_copies[dz, dy].wait_recv()
            to_core(dz, dy)
            pack(dz, dy, 0)

    half = zs * ys * pad
    split = max(1, half // 512)

    def expert(first, count):
        x = packed[first : first + count, :width]
        act = gated(x, gate_w, up_w)
        down = jnp.dot(act, down_w[...], preferred_element_type=F32)
        spread = packed[first : first + count, width:].astype(F32)
        lane = lax.broadcasted_iota(jnp.int32, spread.shape, 1)
        mine = (lane == me) | (lane == me + expert_total)
        return down * jnp.sum(jnp.where(mine, spread, 0.0), axis=1, keepdims=True)

    piece = half // split
    per_piece = zs * ys // split
    for s in range(split):
        near[s * piece : (s + 1) * piece, :] = expert(s * piece, piece)

    for s in range(split):
        for n in range(s * per_piece, (s + 1) * per_piece):
            c_copies[n // ys, n % ys].wait_recv()
            pack(n // ys, n % ys, 1)
        far = expert(half + s * piece, piece)
        for n in range(per_piece):
            core_send[s * per_piece + n] = far[n * pad : n * pad + rows, :].astype(BF16)
        for n in range(s * per_piece, (s + 1) * per_piece):
            sent.append(remote(core_send.at[n], core_recv.at[n], rsc_send_sems.at[n],
                               rsc_recv_sems.at[n], (ep_of(0, 0, 1), tp)))
    c_returns = sent[-zs * ys:]

    def both_cores(dz, dy):
        n = dz * ys + dy
        c_returns[n].wait_recv()
        return near[n * pad : n * pad + rows, :] + core_recv[n].astype(F32)

    order = [dz for dz in range(zs - 1, -1, -1)]
    y_returns = {}
    for dz in order:
        for dy in range(1, ys):
            n = dz * ys + dy
            y_send[n] = both_cores(dz, dy).astype(BF16)
            y_returns[dz, dy] = remote(y_send.at[n], y_recv.at[n], rsy_send_sems.at[n],
                                       rsy_recv_sems.at[n], (ep_of(0, dy, 0), tp))
    z_returns = []
    for dz in order:
        total = both_cores(dz, 0)
        for dy in range(1, ys):
            y_returns[dz, dy].wait_recv()
            total = total + y_recv[dz * ys + dy].astype(F32)
        if dz == 0:
            total = total + shared_part
            for t in range(tps):
                own_share[t] = own_share[t] + total[:, t * share : (t + 1) * share]
        for t in range(tps):
            z_send[dz * tps + t] = total[:, t * share : (t + 1) * share].astype(BF16)
        for dt in range(tps):
            if dz or dt:
                at = dz * tps + dt
                z_returns.append((at, remote(
                    z_send.at[dz * tps + flip(tp, dt)], z_recv.at[at],
                    rsz_send_sems.at[at], rsz_recv_sems.at[at],
                    (ep_of(dz, 0, 0), flip(tp, dt)))))
    result = own_share[tp]
    for at, copy in reversed(z_returns):
        copy.wait_recv()
        result = result + z_recv[at].astype(F32)
    out_ref[...] = result.astype(BF16)

    sent += list(z_copies.values()) + list(y_copies.values()) + list(c_copies.values())
    sent += list(y_returns.values()) + [copy for _, copy in z_returns]
    for copy in sent:
        copy.wait_send()


def per_device(
    ep_count, tp_count,
    tokens, delta_state, mixer_gain, query_weight, key_weight, value_weight,
    write_weight, decay_weight, decay_rate, decay_bias, head_gain, out_weight,
    channel_gain, routes, route_weights, expert_gate, expert_up, expert_down,
    shared_gate, shared_up, shared_down,
):
    rows, width = tokens.shape
    heads, dim = delta_state.shape[1], delta_state.shape[2]
    hidden = expert_gate.shape[2]
    shidden = shared_gate.shape[1]
    chips = ep_count // 2
    ys = 1
    while 4 * ys * ys <= chips:
        ys *= 2
    zs = chips // ys
    extra = round_up(2 * ep_count, 128)
    share = width // tp_count
    vmem = pl.BlockSpec(memory_space=pltpu.VMEM)
    anyspace = pl.BlockSpec(memory_space=pl.ANY)
    dma = pltpu.SemaphoreType.DMA
    chunk = next(c for c in (3, 2, 1) if rows % c == 0)
    column_rows = round_up(2 * heads * round_up(rows, 8), 128)

    next_state, partial, wext = pl.pallas_call(
        functools.partial(mixer_kernel, ep_count, chunk),
        out_shape=(
            jax.ShapeDtypeStruct(delta_state.shape, F32),
            jax.ShapeDtypeStruct((rows, width), BF16),
            jax.ShapeDtypeStruct((rows, extra), BF16),
        ),
        in_specs=[vmem] * 9 + [anyspace] * 5,
        out_specs=(anyspace, vmem, vmem),
        scratch_shapes=[
            pltpu.VMEM(delta_state.shape, F32),
            pltpu.VMEM(query_weight.shape, BF16),
            pltpu.VMEM(key_weight.shape, BF16),
            pltpu.VMEM(value_weight.shape, BF16),
            pltpu.VMEM(out_weight.shape, BF16),
            pltpu.VMEM((column_rows, dim), F32),
            pltpu.VMEM((rows, heads * dim), F32),
            dma((4,)), dma((rows // chunk,)), dma((rows // chunk,)),
        ],
    )(
        tokens, mixer_gain.reshape(1, width), write_weight, decay_weight,
        decay_rate.reshape(1, heads), decay_bias.reshape(1, heads), head_gain.reshape(1, dim),
        routes, route_weights, delta_state, query_weight, key_weight, value_weight, out_weight,
    )

    pad = round_up(rows, 16)
    zy = zs * ys
    layer_out = pl.pallas_call(
        functools.partial(experts_kernel, zs, ys, tp_count, pad),
        out_shape=jax.ShapeDtypeStruct((rows, share), BF16),
        in_specs=[vmem] * 4 + [anyspace] * 6,
        out_specs=vmem,
        scratch_shapes=[
            pltpu.VMEM((width, hidden), BF16), pltpu.VMEM((width, hidden), BF16),
            pltpu.VMEM((hidden, width), BF16),
            pltpu.VMEM((width, shidden), BF16), pltpu.VMEM((width, shidden), BF16),
            pltpu.VMEM((shidden, width), BF16),
            pltpu.VMEM((max(1, tp_count - 1), rows, width), BF16),
            pltpu.VMEM((2 * zy, rows, width + extra), BF16),
            pltpu.VMEM((2 * zy * pad, width + extra), BF16),
            pltpu.VMEM((zy * pad, width), F32),
            pltpu.VMEM((zy, rows, width), BF16), pltpu.VMEM((zy, rows, width), BF16),
            pltpu.VMEM((zy, rows, width), BF16), pltpu.VMEM((zy, rows, width), BF16),
            pltpu.VMEM((zs * tp_count, rows, share), BF16),
            pltpu.VMEM((zs * tp_count, rows, share), BF16),
            pltpu.VMEM((tp_count, rows, share), F32),
            dma((6,)), dma((tp_count,)), dma((tp_count,)),
            dma((zs,)), dma((zs,)), dma((zy,)), dma((zy,)), dma((zy,)), dma((zy,)),
            dma((zy,)), dma((zy,)), dma((zy,)), dma((zy,)),
            dma((zs * tp_count,)), dma((zs * tp_count,)),
        ],
        compiler_params=pltpu.CompilerParams(collective_id=0, has_side_effects=True),
    )(
        tokens, partial, wext, channel_gain.reshape(1, width),
        expert_gate.reshape(width, hidden), expert_up.reshape(width, hidden),
        expert_down.reshape(hidden, width), shared_gate, shared_up, shared_down,
    )
    return layer_out, next_state


def solution(mesh):
    return jax.shard_map(
        functools.partial(per_device, mesh.shape["ep"], mesh.shape["tp"]),
        mesh=mesh,
        in_specs=(
            P("ep", None),
            P("ep", "tp", None, None),
            P(),
            P(None, "tp"),
            P(None, "tp"),
            P(None, "tp"),
            P(None, "tp"),
            P(None, "tp"),
            P("tp"),
            P("tp"),
            P(),
            P("tp", None),
            P(),
            P("ep", None),
            P("ep", None),
            P("ep", None, "tp"),
            P("ep", None, "tp"),
            P("ep", "tp", None),
            P(None, "tp"),
            P(None, "tp"),
            P("tp", None),
        ),
        out_specs=(P("ep", "tp"), P("ep", "tp", None, None)),
        check_vma=False,
    )
```

time: 102 us -> 47.5 us (0.47)
  Pallas kernels: 0 us -> 39.2 us
  blocking collectives: 30.1 us -> 0 us
  waiting for transfers between devices: 24.2 us -> 0 us
  matrix products: 16.6 us -> 0 us
  between operations: 14.4 us -> 0.65 us
  starting transfers between devices: 5.7 us -> 0 us
  other arithmetic: 4.91 us -> 0 us
  local copies, waits for them, and re-layouts: 4.98 us -> 7.2 us
    pallas_call x0 -> x2, Pallas kernels: none -> 39.2 us  [the longest x1 32.5 us: per_device(): pl.pallas_call(functools.partial(experts_kernel, zs, ys, tp_count, pad),...]
    all_to_all x1 -> x0, blocking collectives: 19.9 us -> none  [per_device(): lax.all_to_all(outgoing, 'ep', split_axis=0, concat_axis=0, tiled=True)]
    dot_general x14 -> x0, matrix products: 16.6 us -> none  [the longest x1 2.54 us: per_device(): jnp.einsum('lrf,lfd->lrd', hidden_act, expert_down, preferred_element_typ...]
    reduce_scatter x2 -> x0, waiting for transfers between devices: 15.6 us -> none  [the longest x1 12.3 us: per_device(): lax.psum_scatter(down_part.astype(jnp.bfloat16), 'tp', scatter_dimension=...]
    psum x1 -> x0, blocking collectives: 10.2 us -> none  [per_device(): mixer_out = lax.psum(head_partial.astype(jnp.bfloat16), 'tp')]
    all_to_all x1 -> x0, waiting for transfers between devices: 8.54 us -> none  [per_device(): lax.all_to_all(homeward, 'ep', split_axis=0, concat_axis=0, tiled=True)]
    all_to_all x1 -> x0, starting transfers between devices: 5.62 us -> none  [per_device(): lax.all_to_all(homeward, 'ep', split_axis=0, concat_axis=0, tiled=True)]
    unnamed x25 -> x5, local copies, waits for them, and re-layouts: 2.36 us -> 7.2 us
  transfers between devices with their start and end apart: 3 -> 0, of which waited for: 3 -> 0; matrix products, arithmetic and copies ran while one was open for 1% -> 0% of each run, Pallas kernels for 0% -> 0%
where the time goes in v1:
time: 47.5 us; the launch traced here: 47.1 us
  Pallas kernels  39.2 us (83%)
  local copies, waits for them, and re-layouts  7.2 us (15%)
  between operations  0.65 us (1%)
    pallas_call x1, Pallas kernels, per_device(): pl.pallas_call(functools.partial(experts_kernel, zs, ys, tp_count, pad),...  32.5 us
    unnamed x5, local copies, waits for them, and re-layouts  7.2 us
    pallas_call x1, Pallas kernels, per_device(): pl.pallas_call(functools.partial(mixer_kernel, ep_count, chunk), out_shap...  6.76 us

profile of v1, /device:TPU:0, one launch (start us, length us, event | category | flops | bytes accessed | tf_op | source)
XLA Modules:
  0.0 47.1 jit_solution(7438841758877870569)
XLA Ops:
  0.6 1.4 %copy.25.routes_ref = s32[18,6]{1,0:T(8,128)} copy(s32[18,6]{0,1:T(8,128)} %param.34) | data formatting | bytes 864 | tf_op args[13]
  2.0 1.4 %copy.26.route_weights_ref = f32[18,6]{1,0:T(8,128)} copy(f32[18,6]{0,1:T(8,128)} %param.35) | data formatting | bytes 864 | tf_op args[14]
  3.4 1.6 %copy.23.write_ref = bf16[1024,2]{1,0:T(8,128)(2,1)} copy(bf16[1024,2]{0,1:T(2,128)(2,1)} %param.27) | data formatting | bytes 8192 | tf_op args[6]
  4.9 1.6 %copy.24.decay_ref = bf16[1024,2]{1,0:T(8,128)(2,1)} copy(bf16[1024,2]{0,1:T(2,128)(2,1)} %param.28) | data formatting | bytes 8192 | tf_op args[7]
  6.5 6.8 %shard_map.212 = (f32[18,2,128,128]{3,2,1,0:T(8,128)}, bf16[18,1024]{1,0:T(8,128)(2,1)}, bf16[18,128]{1,0:T(8,128)(2,1)}) custom-call(bf16[18,1024]{1,0:T(8,128)(2,1)} %tokens_ref.3, f32[1,1024]{1,0:T(1,128)} %bitcast.11, bf16[1024,2]{1,0:T(8,128)(2,1)} %copy.23.write_ref, bf16[1024,2]{1,0:T(8,128)(2,1)} %copy.24.decay_ref, f32[1,2]{1,0:T(1,128)} %bitcast.13, ...), custom_call_target="tpu_custom_call" | custom-call | tf_op jit(solution)/shard_map/pallas_call | solution.py:361
  13.3 32.5 %shard_map.213 = bf16[18,512]{1,0:T(8,128)(2,1)} custom-call(bf16[18,1024]{1,0:T(8,128)(2,1)} %tokens_ref.3, bf16[18,1024]{1,0:T(8,128)(2,1)} %get-tuple-element.5.partial_ref, bf16[18,128]{1,0:T(8,128)(2,1)} %get-tuple-element.6.wext_ref, f32[1,1024]{1,0:T(1,128)} %bitcast.12, bf16[1024,256]{1,0:T(8,128)(2,1)} %bitcast.8, bf16[1024,256]{1,0:T(8,128)(2,1)} %bitcast.9, ...), custom_call_target="tpu_custom_call" | custom-call | tf_op jit(solution)/shard_map/pallas_call | solution.py:388
  45.7 1.3 %copy.28 = bf16[18,512]{1,0:T(8,128)(2,1)} copy(bf16[18,512]{1,0:T(8,128)(2,1)} %shard_map.213) | data formatting | bytes 36864

commit v2 on v1

--- a/solution.py
+++ b/solution.py
@@ -29,7 +29,7 @@
     head_gain_ref, routes_ref, route_weights_ref,
     state_hbm, query_hbm, key_hbm, value_hbm, out_hbm,
     next_hbm, partial_ref, wext_ref,
-    state, query_w, key_w, value_w, out_w, columns, readout,
+    state, query_w, key_w, value_w, out_w, columns, readout, spread,
     weight_sems, in_sems, out_sems,
 ):
     rows, heads, dim = state.shape[0], state.shape[1], state.shape[2]
@@ -56,22 +56,31 @@
         copy.start()
 
     raw = route_weights_ref[...]
-    norm = raw / jnp.sum(raw, axis=1, keepdims=True) * ROUTED_SCALE
+    norm = raw / jnp.sum(raw, axis=0, keepdims=True) * ROUTED_SCALE
     routes = routes_ref[...]
-    lane = lax.broadcasted_iota(jnp.int32, (rows, wext_ref.shape[1]), 1)
-    high = jnp.zeros(lane.shape, F32)
-    for k in range(routes.shape[1]):
-        hit = (lane == routes[:, k : k + 1]) | (lane == routes[:, k : k + 1] + expert_total)
-        high = high + jnp.where(hit, norm[:, k : k + 1], 0.0)
-    rounded = high.astype(BF16)
-    low = (high - rounded.astype(F32)).astype(BF16)
-    wext_ref[...] = jnp.where(lane < expert_total, rounded.astype(F32), low.astype(F32)).astype(BF16)
+    row = lax.broadcasted_iota(jnp.int32, (spread.shape[0], rows), 0)
+    high = jnp.zeros(row.shape, F32)
+    for k in range(routes.shape[0]):
+        named = routes[k : k + 1, :]
+        hit = (row == named) | (row == named + expert_total)
+        high = high + jnp.where(hit, norm[k : k + 1, :], 0.0)
+    rounded = high.astype(BF16).astype(F32)
+    spread[:, :rows] = jnp.where(row < expert_total, rounded, high - rounded)
+    wext_ref[...] = spread[...].T[:rows, :].astype(BF16)
 
     normed = rms_rows(tokens_ref[...].astype(F32), mixer_gain_ref[...]).astype(BF16)
-    write_rate = jax.nn.sigmoid(jnp.dot(normed, write_ref[...], preferred_element_type=F32))
-    pre = jnp.dot(normed, decay_ref[...], preferred_element_type=F32) + bias_ref[...]
-    softplus = jnp.maximum(pre, 0.0) + jnp.log1p(jnp.exp(-jnp.abs(pre)))
-    keep = jnp.exp(-rate_ref[...] * softplus)
+    wide = normed.astype(F32)
+
+    def per_head_dot(ref):
+        table = ref[...].astype(F32)
+        return [jnp.sum(wide * table[h : h + 1, :], axis=-1, keepdims=True) for h in range(heads)]
+
+    write_rate = [jax.nn.sigmoid(x) for x in per_head_dot(write_ref)]
+    keep = []
+    for h, pre in enumerate(per_head_dot(decay_ref)):
+        pre = pre + bias_ref[:, h : h + 1]
+        softplus = jnp.maximum(pre, 0.0) + jnp.log1p(jnp.exp(-jnp.abs(pre)))
+        keep.append(jnp.exp(-rate_ref[:, h : h + 1] * softplus))
 
     def project(copy, ref):
         copy.wait()
@@ -93,8 +102,8 @@
         per_head.append(
             (
                 value_raw[:, part],
-                jnp.broadcast_to(keep[:, h : h + 1], (rows, dim)),
-                jnp.broadcast_to(write_rate[:, h : h + 1], (rows, dim)),
+                jnp.broadcast_to(keep[h], (rows, dim)),
+                jnp.broadcast_to(write_rate[h], (rows, dim)),
                 jnp.broadcast_to(dots, (rows, dim)),
             )
         )
@@ -208,12 +217,13 @@
     blocks[0, :, width:] = wext_ref[...]
 
     def slot(dz, dy, dc):
-        return (dc * zs + dz) * ys + dy
-
+        return (dz * 2 + dc) * ys + dy
+
+    order = [0] + list(range(zs - 1, 0, -1))
     z_copies = {
         dz: remote(blocks.at[slot(0, 0, 0)], blocks.at[slot(dz, 0, 0)],
                    agz_send_sems.at[dz], agz_recv_sems.at[dz], (ep_of(dz, 0, 0), tp))
-        for dz in range(1, zs)
+        for dz in order[1:]
     }
     y_copies, c_copies = {}, {}
 
@@ -247,67 +257,59 @@
 
     shared_act = gated(expert_input, sgate_w, sup_w)
     shared_part = jnp.dot(shared_act, sdown_w[...], preferred_element_type=F32)
-    pack(0, 0, 0)
     for copy in weights[3:]:
         copy.wait()
 
-    for dz in range(1, zs):
-        z_copies[dz].wait_recv()
-        pass_on(dz)
+    def gather_z(dz):
+        if dz:
+            z_copies[dz].wait_recv()
+            pass_on(dz)
         pack(dz, 0, 0)
-    for dz in range(zs):
+
+    def gather_y(dz):
         for dy in range(1, ys):
             y_copies[dz, dy].wait_recv()
             to_core(dz, dy)
             pack(dz, dy, 0)
 
-    half = zs * ys * pad
-    split = max(1, half // 512)
-
-    def expert(first, count):
-        x = packed[first : first + count, :width]
+    half = ys * pad
+    c_returns, y_returns, z_returns = {}, {}, []
+
+    def run_expert(dz):
+        for dy in range(ys):
+            c_copies[dz, dy].wait_recv()
+            pack(dz, dy, 1)
+        first = slot(dz, 0, 0) * pad
+        x = packed[first : first + 2 * half, :width]
         act = gated(x, gate_w, up_w)
         down = jnp.dot(act, down_w[...], preferred_element_type=F32)
-        spread = packed[first : first + count, width:].astype(F32)
+        spread = packed[first : first + 2 * half, width:].astype(F32)
         lane = lax.broadcasted_iota(jnp.int32, spread.shape, 1)
         mine = (lane == me) | (lane == me + expert_total)
-        return down * jnp.sum(jnp.where(mine, spread, 0.0), axis=1, keepdims=True)
-
-    piece = half // split
-    per_piece = zs * ys // split
-    for s in range(split):
-        near[s * piece : (s + 1) * piece, :] = expert(s * piece, piece)
-
-    for s in range(split):
-        for n in range(s * per_piece, (s + 1) * per_piece):
-            c_copies[n // ys, n % ys].wait_recv()
-            pack(n // ys, n % ys, 1)
-        far = expert(half + s * piece, piece)
-        for n in range(per_piece):
-            core_send[s * per_piece + n] = far[n * pad : n * pad + rows, :].astype(BF16)
-        for n in range(s * per_piece, (s + 1) * per_piece):
-            sent.append(remote(core_send.at[n], core_recv.at[n], rsc_send_sems.at[n],
-                               rsc_recv_sems.at[n], (ep_of(0, 0, 1), tp)))
-    c_returns = sent[-zs * ys:]
+        down = down * jnp.sum(jnp.where(mine, spread, 0.0), axis=1, keepdims=True)
+        for dy in range(ys - 1, -1, -1):
+            n = dz * ys + dy
+            core_send[n] = down[half + dy * pad : half + dy * pad + rows, :].astype(BF16)
+            c_returns[n] = remote(core_send.at[n], core_recv.at[n], rsc_send_sems.at[n],
+                                  rsc_recv_sems.at[n], (ep_of(0, 0, 1), tp))
+        near[dz * half : (dz + 1) * half, :] = down[:half, :]
 
     def both_cores(dz, dy):
         n = dz * ys + dy
         c_returns[n].wait_recv()
         return near[n * pad : n * pad + rows, :] + core_recv[n].astype(F32)
 
-    order = [dz for dz in range(zs - 1, -1, -1)]
-    y_returns = {}
-    for dz in order:
+    def return_y(dz):
         for dy in range(1, ys):
             n = dz * ys + dy
             y_send[n] = both_cores(dz, dy).astype(BF16)
-            y_returns[dz, dy] = remote(y_send.at[n], y_recv.at[n], rsy_send_sems.at[n],
-                                       rsy_recv_sems.at[n], (ep_of(0, dy, 0), tp))
-    z_returns = []
-    for dz in order:
+            y_returns[n] = remote(y_send.at[n], y_recv.at[n], rsy_send_sems.at[n],
+                                  rsy_recv_sems.at[n], (ep_of(0, dy, 0), tp))
+
+    def return_z(dz):
         total = both_cores(dz, 0)
         for dy in range(1, ys):
-            y_returns[dz, dy].wait_recv()
+            y_returns[dz * ys + dy].wait_recv()
             total = total + y_recv[dz * ys + dy].astype(F32)
         if dz == 0:
             total = total + shared_part
@@ -315,21 +317,27 @@
                 own_share[t] = own_share[t] + total[:, t * share : (t + 1) * share]
         for t in range(tps):
             z_send[dz * tps + t] = total[:, t * share : (t + 1) * share].astype(BF16)
-        for dt in range(tps):
+        for dt in range(tps - 1, -1, -1):
             if dz or dt:
                 at = dz * tps + dt
                 z_returns.append((at, remote(
                     z_send.at[dz * tps + flip(tp, dt)], z_recv.at[at],
                     rsz_send_sems.at[at], rsz_recv_sems.at[at],
                     (ep_of(dz, 0, 0), flip(tp, dt)))))
+
+    stages = (gather_z, gather_y, run_expert, return_y, return_z)
+    for step in range(zs + len(stages) - 1):
+        for lag, stage in enumerate(stages):
+            if 0 <= step - lag < zs:
+                stage(order[step - lag])
     result = own_share[tp]
-    for at, copy in reversed(z_returns):
+    for at, copy in z_returns:
         copy.wait_recv()
         result = result + z_recv[at].astype(F32)
     out_ref[...] = result.astype(BF16)
 
     sent += list(z_copies.values()) + list(y_copies.values()) + list(c_copies.values())
-    sent += list(y_returns.values()) + [copy for _, copy in z_returns]
+    sent += list(c_returns.values()) + list(y_returns.values()) + [copy for _, copy in z_returns]
     for copy in sent:
         copy.wait_send()
 
@@ -375,12 +383,13 @@
             pltpu.VMEM(out_weight.shape, BF16),
             pltpu.VMEM((column_rows, dim), F32),
             pltpu.VMEM((rows, heads * dim), F32),
+            pltpu.VMEM((extra, round_up(rows, 128)), F32),
             dma((4,)), dma((rows // chunk,)), dma((rows // chunk,)),
         ],
     )(
-        tokens, mixer_gain.reshape(1, width), write_weight, decay_weight,
+        tokens, mixer_gain.reshape(1, width), write_weight.T, decay_weight.T,
         decay_rate.reshape(1, heads), decay_bias.reshape(1, heads), head_gain.reshape(1, dim),
-        routes, route_weights, delta_state, query_weight, key_weight, value_weight, out_weight,
+        routes.T, route_weights.T, delta_state, query_weight, key_weight, value_weight, out_weight,
     )
 
     pad = round_up(rows, 16)

time: 47.5 us -> 41.1 us (0.87)
  local copies, waits for them, and re-layouts: 7.2 us -> 1.35 us
    unnamed x5 -> x1, local copies, waits for them, and re-layouts: 7.2 us -> 1.35 us
where the time goes in v2:
time: 41.1 us; the launch traced here: 40.8 us
  Pallas kernels  38.8 us (94%)
  local copies, waits for them, and re-layouts  1.35 us (3%)
  between operations  0.65 us (2%)
    pallas_call x1, Pallas kernels, per_device(): pl.pallas_call(functools.partial(experts_kernel, zs, ys, tp_count, pad),...  32.2 us
    pallas_call x1, Pallas kernels, per_device(): pl.pallas_call(functools.partial(mixer_kernel, ep_count, chunk), out_shap...  6.54 us
    unnamed x1, local copies, waits for them, and re-layouts  1.35 us

profile of v2, /device:TPU:0, one launch (start us, length us, event | category | flops | bytes accessed | tf_op | source)
XLA Modules:
  0.0 40.8 jit_solution(12543279571326582641)
XLA Ops:
  0.6 6.5 %shard_map.212 = (f32[18,2,128,128]{3,2,1,0:T(8,128)}, bf16[18,1024]{1,0:T(8,128)(2,1)}, bf16[18,128]{1,0:T(8,128)(2,1)}) custom-call(bf16[18,1024]{1,0:T(8,128)(2,1)} %tokens_ref.3, f32[1,1024]{1,0:T(1,128)} %bitcast.15, bf16[2,1024]{1,0:T(2,128)(2,1)} %bitcast.16, bf16[2,1024]{1,0:T(2,128)(2,1)} %bitcast.17, f32[1,2]{1,0:T(1,128)} %bitcast.21, ...), custom_call_target="tpu_custom_call" | custom-call | tf_op jit(solution)/shard_map/pallas_call | solution.py:369
  7.2 32.2 %shard_map.213 = bf16[18,512]{1,0:T(8,128)(2,1)} custom-call(bf16[18,1024]{1,0:T(8,128)(2,1)} %tokens_ref.3, bf16[18,1024]{1,0:T(8,128)(2,1)} %get-tuple-element.5.partial_ref, bf16[18,128]{1,0:T(8,128)(2,1)} %get-tuple-element.6.wext_ref, f32[1,1024]{1,0:T(1,128)} %bitcast.20, bf16[1024,256]{1,0:T(8,128)(2,1)} %bitcast.12, bf16[1024,256]{1,0:T(8,128)(2,1)} %bitcast.13, ...), custom_call_target="tpu_custom_call" | custom-call | tf_op jit(solution)/shard_map/pallas_call | solution.py:397
  39.4 1.3 %copy.24 = bf16[18,512]{1,0:T(8,128)(2,1)} copy(bf16[18,512]{1,0:T(8,128)(2,1)} %shard_map.213) | data formatting | bytes 36864
